TPU v7x, 32 devices: a whole 2x2x4 slice. The times are simulated.
32 devices in a mesh: sp: 16 (over z, y, x), tp: 2 (over core).
Axes of the slice: x: 2, y: 2, z: 4, core: 2. Of those that a mesh axis runs over, the one named last changes fastest.
Arguments:
- tokens_in: bfloat16 [2048, 2048], P(('sp', 'tp')), may hold values from -9 to 9, as said below
- w_query: bfloat16 [2048, 2048], P(None, 'tp'), may hold values from -0.125 to 0.125
- w_key: bfloat16 [2048, 512], P(None, 'tp'), may hold values from -0.125 to 0.125
- w_value: bfloat16 [2048, 512], P(None, 'tp'), may hold values from -0.125 to 0.125
- w_out: bfloat16 [2048, 2048], P('tp'), may hold values from -0.125 to 0.125
- q_gain: float32 [64], replicated, may hold values from 0.1 to 14
- k_gain: float32 [64], replicated, may hold values from 0.1 to 14
Outputs:
- attended: bfloat16 [2048, 2048], P(('sp', 'tp'))
Inputs may be any that keep to these rules, and one draw needn't show every extreme that they name: `tokens_in`: activations whose mean differs from one block of 128 tokens to another.
All inputs are finite; a program needn't handle non-finite values.
Results may differ from a plain program's by a relative error of at most 0.014.
The roundings to bfloat16 on the way count: a program that leaves them out, or rounds other values in their place, can miss the bound.
Values may be sent and summed in bfloat16 or wider, within the bound.
A program may use at most 64 MiB of HBM per device.

v0:
```python
import jax
import jax.numpy as jnp
from jax import lax
from jax.sharding import PartitionSpec as P

GRID_W = 64


def turned(vectors, position, gain):
    pairs = vectors.shape[-1] // 4
    scaled = vectors * lax.rsqrt(jnp.mean(vectors * vectors, axis=-1, keepdims=True) + 1e-06) * gain
    freq = 10000.0 ** (-jnp.arange(pairs, dtype=jnp.float32) / pairs)
    grid_row = (position // GRID_W).astype(jnp.float32)
    grid_col = (position % GRID_W).astype(jnp.float32)
    angle = jnp.stack([grid_row[:, None] * freq, grid_col[:, None] * freq], axis=1)
    cosine = jnp.cos(angle)[:, None]
    sine = jnp.sin(angle)[:, None]
    split = scaled.reshape(scaled.shape[:-1] + (2, 2, pairs))
    first = split[..., 0, :]
    second = split[..., 1, :]
    joined = jnp.stack([first * cosine - second * sine, first * sine + second * cosine], axis=-2)
    return joined.reshape(scaled.shape)


def body(tokens_in, w_query, w_key, w_value, w_out, q_gain, k_gain):
    head_dim = q_gain.shape[0]
    query_cols = w_query.shape[1]
    key_cols = w_key.shape[1]
    kv_heads = key_cols // head_dim
    group = query_cols // key_cols
    w_joined = jnp.concatenate([w_query, w_key, w_value], axis=1)
    projected = jnp.dot(
        lax.all_gather(tokens_in, "tp", axis=0, tiled=True),
        w_joined,
        preferred_element_type=jnp.float32,
    ).astype(jnp.bfloat16)
    row_count = projected.shape[0]
    position = lax.axis_index("sp") * row_count + jnp.arange(row_count, dtype=jnp.int32)
    query_n = turned(
        projected[:, :query_cols]
        .astype(jnp.float32)
        .reshape(row_count, kv_heads * group, head_dim),
        position,
        q_gain,
    ).astype(jnp.bfloat16)
    query_g = query_n.reshape(row_count, kv_heads, group, head_dim).transpose(1, 2, 0, 3)
    raw_keys = projected[:, query_cols : query_cols + key_cols]
    values = projected[:, query_cols + key_cols :]
    scale = head_dim ** (-0.5)
    outgoing = jnp.concatenate([raw_keys, values], axis=1)
    piece = lax.all_gather(outgoing, "sp", axis=0, tiled=True)
    length = piece.shape[0]
    spot = jnp.arange(length, dtype=jnp.int32)
    keys_n = turned(
        piece[:, :key_cols].astype(jnp.float32).reshape(length, kv_heads, head_dim), spot, k_gain
    ).astype(jnp.bfloat16)
    peak = jnp.full((kv_heads, group, row_count), -1e30, jnp.float32)
    scores = (
        jnp.einsum("kgqd,nkd->kgqn", query_g, keys_n, preferred_element_type=jnp.float32) * scale
    )
    new_peak = jnp.maximum(peak, jnp.max(scores, axis=-1))
    expo = jnp.exp(scores - new_peak[..., None])
    total = jnp.sum(expo, axis=-1)
    summed = jnp.einsum(
        "kgqn,nkd->kgqd",
        expo.astype(jnp.bfloat16),
        piece[:, key_cols:].reshape(length, kv_heads, head_dim),
        preferred_element_type=jnp.float32,
    )
    peak, total, summed = (new_peak, total, summed)
    mixed = (summed / total[..., None]).astype(jnp.bfloat16)
    mixed = mixed.transpose(2, 0, 1, 3).reshape(row_count, query_cols)
    return lax.psum_scatter(
        jnp.dot(mixed, w_out, preferred_element_type=jnp.float32).astype(jnp.bfloat16),
        "tp",
        scatter_dimension=0,
        tiled=True,
    )


def solution(mesh):
    return jax.shard_map(
        body,
        mesh=mesh,
        in_specs=(
            P(("sp", "tp"), None),
            P(None, "tp"),
            P(None, "tp"),
            P(None, "tp"),
            P("tp", None),
            P(),
            P(),
        ),
        out_specs=P(("sp", "tp"), None),
        check_vma=False,
    )
```

profile of v0, /device:TPU:0, one launch (start us, length us, event | category | flops | bytes accessed | tf_op | source)
XLA Modules:
  0.0 117.6 jit_solution(13708748384121845471)
XLA Ops:
  6.5 2.5 %all_gather.6 = bf16[128,2048]{1,0:T(8,128)(2,1)S(1)} all-gather(bf16[64,2048]{1,0:T(8,128)(2,1)} %param.7), channel_id=1, replica_groups=mesh['sp'=16,'tp'=2] {'tp'}, dimensions={0}, use_global_device_ids=true | all-gather | bytes 786432 | tf_op jit(solution)/shard_map/all_gather | solution.py:33
  9.0 4.1 %fusion.13 = bf16[128,1536]{0,1:T(8,128)(2,1)S(1)} fusion(bf16[128,2048]{1,0:T(8,128)(2,1)S(1)} %all_gather.6, bf16[2048,256]{1,0:T(8,128)(2,1)} %param.10, bf16[2048,256]{1,0:T(8,128)(2,1)} %param.9, bf16[2048,1024]{1,0:T(8,128)(2,1)} %param.8), kind=kOutput, calls=%fused_computation.13 | convolution fusion | flops 824377344 | bytes 7208960 | tf_op jit(solution)/shard_map/dot_general | solution.py:32
  13.1 0.7 concatenate.24
  13.9 0.1 mul.221
  13.9 0.1 mul.240
  14.1 0.1 broadcast_multiply_fusion.3
  14.1 0.1 fusion.34
  14.2 0.1 bitcast_reduce_fusion.1
  14.4 0.1 multiply_multiply_fusion.1
  14.5 0.1 subtract_convert_fusion.1
  14.6 0.1 broadcast_multiply_fusion.1
  14.7 1.0 fusion.27
  15.7 63.8 %all-gather.2.cloned.1.call-done = bf16[2048,512]{0,1:T(8,128)(2,1)} async-done(((bf16[128,512]{0,1:T(8,128)(2,1)}), bf16[2048,512]{0,1:T(8,128)(2,1)}) %all-gather.2.cloned.1.call-update) | async-done | bytes 2097168 | tf_op jit(solution)/shard_map/all_gather | solution.py:51
  79.5 1.5 %bitcast_reduce_fusion = f32[2048,4]{0,1:T(4,128)S(1)} fusion(bf16[2048,512]{0,1:T(8,128)(2,1)} %all-gather.2.cloned.1.call-done), kind=kLoop, calls=%fused_computation.14 | loop fusion | flops 1564672 | bytes 1081344 | tf_op jit(solution)/shard_map/reduce_sum | solution.py:11
  81.0 1.8 %slice_convert_fusion = (f32[2048,256]{0,1:T(8,128)S(1)}, bf16[2048,256]{0,1:T(8,128)(2,1)S(1)}) fusion(bf16[2048,512]{0,1:T(8,128)(2,1)} %all-gather.2.cloned.1.call-done), kind=kLoop, calls=%fused_computation.17 | loop fusion | flops 524288 | bytes 5242880 | tf_op jit(solution)/shard_map/convert_element_type | solution.py:55
  82.9 0.4 multiply_multiply_fusion
  83.3 0.3 subtract_convert_fusion
  83.6 0.1 pad_maximum_fusion
  83.7 2.5 %multiply_reduce_fusion = (f32[4,4,128]{2,1,0:T(4,128)S(1)}, f32[4,4,128,2048]{3,2,1,0:T(8,128)S(1)}) fusion(bf16[4,4,128,64]{2,3,1,0:T(8,128)(2,1)S(1)} %bitcast.38, bf16[2048,4,64,1]{0,2,3,1:T(8,128)(2,1)S(1)} %bitcast.36), kind=kOutput, calls=%fused_computation.1 | convolution fusion | flops 545257472 | bytes 18096128 | tf_op jit(solution)/shard_map/kgqd,nkd->kgqn/dot_general | solution.py:59
  86.2 3.3 %fusion = f32[4,4,128]{2,1,0:T(4,128)S(1)} fusion(f32[4,4,128,2048]{3,2,1,0:T(8,128)S(1)} %get-tuple-element.20, f32[4,4,128]{2,1,0:T(4,128)S(1)} %broadcast_maximum_fusion), kind=kLoop, calls=%fused_computation.2 | loop fusion | flops 12580864 | bytes 16793600 | tf_op jit(solution)/shard_map/reduce_sum | solution.py:63
  89.5 2.4 %copy-done = f32[4,4,128,2048]{3,2,1,0:T(8,128)} copy-done((f32[4,4,128,2048]{3,2,1,0:T(8,128)}, f32[4,4,128,2048]{3,2,1,0:T(8,128)S(1)}, u32[]{:S(2)}) %copy-start) | copy-done | bytes 16777240
  91.9 8.8 %fusion.22 = bf16[128,4,4,64]{0,3,2,1:T(8,128)(2,1)S(1)} fusion(bf16[2048,4,64,1]{0,2,3,1:T(8,128)(2,1)S(1)} %bitcast.39, f32[4,4,128,2048]{3,2,1,0:T(8,128)} %copy-done, f32[4,4,128]{2,1,0:T(4,128)S(1)} %broadcast_maximum_fusion, f32[128,4,4]{0,2,1:T(4,128)S(1)} %bitcast.41), kind=kOutput, calls=%fused_computation.22 | convolution fusion | flops 549715968 | bytes 18104320 | tf_op jit(solution)/shard_map/kgqn,nkd->kgqd/dot_general | solution.py:64
  100.8 3.7 %convolution_convert_fusion = bf16[128,2048]{1,0:T(8,128)(2,1)} fusion(bf16[128,1024]{0,1:T(8,128)(2,1)S(1)} %bitcast.40, bf16[1024,2048]{1,0:T(8,128)(2,1)} %param.11), kind=kOutput, calls=%fused_computation.12 | convolution fusion | flops 537133056 | bytes 4980736 | tf_op jit(solution)/shard_map/dot_general | solution.py:74
  104.5 6.3 %reduce-scatter.2.cloned.1.call-done = bf16[64,2048]{1,0:T(8,128)(2,1)} async-done(((bf16[128,2048]{1,0:T(8,128)(2,1)}), bf16[64,2048]{1,0:T(8,128)(2,1)}) %reduce-scatter.2.cloned.1.call-update) | async-done | bytes 262160 | tf_op jit(solution)/shard_map/reduce_scatter | solution.py:73
  (17 shorter events, 0.2 us)
Async XLA Ops:
  6.5 73.0 %all-gather.2.cloned.1.call-start = ((), (), s32[]{:S(2)}) async-start(), calls=%async_computation.1 | async-start | bytes 2228224 | tf_op jit(solution)/shard_map/all_gather | solution.py:51
  9.0 4.8 %copy-start.1 = (f32[64]{0:T(128)S(1)}, f32[64]{0:T(128)}, u32[]{:S(2)}) copy-start(f32[64]{0:T(128)} %param.12) | copy-start | bytes 772
  9.0 4.9 %copy-start.2 = (f32[64]{0:T(128)S(1)}, f32[64]{0:T(128)}, u32[]{:S(2)}) copy-start(f32[64]{0:T(128)} %param.13) | copy-start | bytes 772
  13.8 97.0 %reduce-scatter.2.cloned.1.call-start = ((), (), s32[]{:S(2)}) async-start(), calls=%async_computation.2 | async-start | bytes 786432 | tf_op jit(solution)/shard_map/reduce_scatter | solution.py:73
  86.2 5.7 %copy-start = (f32[4,4,128,2048]{3,2,1,0:T(8,128)}, f32[4,4,128,2048]{3,2,1,0:T(8,128)S(1)}, u32[]{:S(2)}) copy-start(f32[4,4,128,2048]{3,2,1,0:T(8,128)S(1)} %get-tuple-element.20) | copy-start | bytes 50331652
Sparse Core Ops, SparseCore 0:
  13.9 65.5 all-gather.1
  104.6 6.0 reduce-scatter.1
where the time goes:
time: 118 us
  waiting for transfers between devices  70.1 us (59%)
  matrix products  19.1 us (16%)
  between operations  13.6 us (12%)
  other arithmetic  9.04 us (8%)
  local copies, waits for them, and re-layouts  3.27 us (3%)
  blocking collectives  2.5 us (2%)
    all_gather x1, waiting for transfers between devices, body(): piece = lax.all_gather(outgoing, 'sp', axis=0, tiled=True)  63.8 us
    dot_general x1, matrix products, body(): jnp.einsum('kgqn,nkd->kgqd', expo.astype(jnp.bfloat16), piece[:, key_cols...  8.83 us
    reduce_scatter x1, waiting for transfers between devices, body(): lax.psum_scatter(jnp.dot(mixed, w_out, preferred_element_type=jnp.float32...  6.26 us
    dot_general x1, matrix products, body(): jnp.dot(lax.all_gather(tokens_in, 'tp', axis=0, tiled=True), w_joined, pr...  4.06 us
    dot_general x1, matrix products, body(): jnp.dot(mixed, w_out, preferred_element_type=jnp.float32)  3.73 us
    reduce_sum x1, other arithmetic, body(): total = jnp.sum(expo, axis=-1)  3.27 us
    all_gather x1, blocking collectives, body(): lax.all_gather(tokens_in, 'tp', axis=0, tiled=True)  2.5 us
    dot_general x1, matrix products, body(): jnp.einsum('kgqd,nkd->kgqn', query_g, keys_n, preferred_element_type=jnp....  2.47 us
  transfers between devices with their start and end apart: 2, of which 2 were waited for; matrix products, arithmetic and copies ran while one was open for 1% of the time, Pallas kernels for 0%

commit v1 on v0

--- a/solution.py
+++ b/solution.py
@@ -48,7 +48,12 @@
     values = projected[:, query_cols + key_cols :]
     scale = head_dim ** (-0.5)
     outgoing = jnp.concatenate([raw_keys, values], axis=1)
-    piece = lax.all_gather(outgoing, "sp", axis=0, tiled=True)
+    ring = [outgoing]
+    for hop in range(15):
+        ring.append(lax.ppermute(ring[-1], "sp", [(dev, (dev + 1) % 16) for dev in range(16)]))
+    piece = jnp.roll(
+        jnp.concatenate(ring[::-1], axis=0), (lax.axis_index("sp") + 1) * ring[0].shape[0], axis=0
+    )
     length = piece.shape[0]
     spot = jnp.arange(length, dtype=jnp.int32)
     keys_n = turned(

time: 118 us -> 180 us (1.53)
  waiting for transfers between devices: 70.1 us -> 132 us
  starting transfers between devices: 0.04 us -> 2.94 us
  other arithmetic: 9.04 us -> 6.26 us
    ppermute x0 -> x15, waiting for transfers between devices: none -> 128 us  [body(): lax.ppermute(ring[-1], 'sp', [(dev, (dev + 1) % 16) for dev in range(16)])]
    all_gather x1 -> x0, waiting for transfers between devices: 63.8 us -> none  [body(): piece = lax.all_gather(outgoing, 'sp', axis=0, tiled=True)]
    ppermute x0 -> x15, starting transfers between devices: none -> 2.94 us  [body(): lax.ppermute(ring[-1], 'sp', [(dev, (dev + 1) % 16) for dev in range(16)])]
    reduce_scatter x1, waiting for transfers between devices: 6.26 us -> 3.96 us  [body(): lax.psum_scatter(jnp.dot(mixed, w_out, preferred_element_type=jnp.float32...]
    unnamed x6 -> x37, local copies, waits for them, and re-layouts: 2.44 us -> 3.68 us
  transfers between devices with their start and end apart: 2 -> 16, of which waited for: 2 -> 16; matrix products, arithmetic and copies ran while one was open for 1% -> 1% of each run, Pallas kernels for 0% -> 0%
where the time goes in v1:
time: 180 us
  waiting for transfers between devices  132 us (73%)
  matrix products  19 us (11%)
  between operations  13.8 us (8%)
  other arithmetic  6.26 us (3%)
  local copies, waits for them, and re-layouts  3.9 us (2%)
  starting transfers between devices  2.94 us (2%)
  blocking collectives  2.5 us (1%)
    ppermute x15, waiting for transfers between devices, body(): lax.ppermute(ring[-1], 'sp', [(dev, (dev + 1) % 16) for dev in range(16)])  128 us
    dot_general x1, matrix products, body(): jnp.einsum('kgqn,nkd->kgqd', expo.astype(jnp.bfloat16), piece[:, key_cols...  8.8 us
    dot_general x1, matrix products, body(): jnp.dot(lax.all_gather(tokens_in, 'tp', axis=0, tiled=True), w_joined, pr...  4.02 us
    reduce_scatter x1, waiting for transfers between devices, body(): lax.psum_scatter(jnp.dot(mixed, w_out, preferred_element_type=jnp.float32...  3.96 us
    dot_general x1, matrix products, body(): jnp.dot(mixed, w_out, preferred_element_type=jnp.float32)  3.73 us
    unnamed x37, local copies, waits for them, and re-layouts  3.68 us
  transfers between devices with their start and end apart: 16, of which 16 were waited for; matrix products, arithmetic and copies ran while one was open for 1% of the time, Pallas kernels for 0%

profile of v1, /device:TPU:0, one launch (start us, length us, event | category | flops | bytes accessed | tf_op | source)
XLA Modules:
  0.0 180.3 jit_solution(16063612081057657763)
XLA Ops:
  6.5 2.5 %all_gather.3 = bf16[128,2048]{1,0:T(8,128)(2,1)S(1)} all-gather(bf16[64,2048]{1,0:T(8,128)(2,1)} %param.7), channel_id=1, replica_groups=mesh['sp'=16,'tp'=2] {'tp'}, dimensions={0}, use_global_device_ids=true | all-gather | bytes 786432 | tf_op jit(solution)/shard_map/all_gather | solution.py:33
  9.0 4.0 %fusion.13 = bf16[128,1536]{0,1:T(8,128)(2,1)S(1)} fusion(bf16[128,2048]{1,0:T(8,128)(2,1)S(1)} %all_gather.3, bf16[2048,256]{1,0:T(8,128)(2,1)} %param.10, bf16[2048,256]{1,0:T(8,128)(2,1)} %param.9, bf16[2048,1024]{1,0:T(8,128)(2,1)} %param.8), kind=kOutput, calls=%fused_computation.13 | convolution fusion | flops 824377344 | bytes 7208960 | tf_op jit(solution)/shard_map/dot_general | solution.py:32
  13.1 2.9 %collective-permute-start = (bf16[128,512]{0,1:T(8,128)(2,1)S(1)}, bf16[128,512]{0,1:T(8,128)(2,1)S(1)}, u32[]{:S(2)}, u32[]{:S(2)}) collective-permute-start(bf16[128,512]{0,1:T(8,128)(2,1)S(1)} %concatenate.31), channel_id=1, source_target_pairs={{0,2},{2,4},{4,6},{6,8},{8,10},{10,12},{12,14},{14,16},{16,18},{18... | collective-permute-start | bytes 393224 | tf_op jit(solution)/shard_map/ppermute | solution.py:53
  16.0 7.8 %collective-permute-done = bf16[128,512]{0,1:T(8,128)(2,1)S(1)} collective-permute-done((bf16[128,512]{0,1:T(8,128)(2,1)S(1)}, bf16[128,512]{0,1:T(8,128)(2,1)S(1)}, u32[]{:S(2)}, u32[]{:S(2)}) %collective-permute-start) | collective-permute-done | bytes 131104 | tf_op jit(solution)/shard_map/ppermute | solution.py:53
  23.8 8.6 %collective-permute-done.1 = bf16[128,512]{0,1:T(8,128)(2,1)S(1)} collective-permute-done((bf16[128,512]{0,1:T(8,128)(2,1)S(1)}, bf16[128,512]{0,1:T(8,128)(2,1)S(1)}, u32[]{:S(2)}, u32[]{:S(2)}) %collective-permute-start.1) | collective-permute-done | bytes 131104 | tf_op jit(solution)/shard_map/ppermute | solution.py:53
  32.4 8.6 %collective-permute-done.2 = bf16[128,512]{0,1:T(8,128)(2,1)S(1)} collective-permute-done((bf16[128,512]{0,1:T(8,128)(2,1)S(1)}, bf16[128,512]{0,1:T(8,128)(2,1)S(1)}, u32[]{:S(2)}, u32[]{:S(2)}) %collective-permute-start.2) | collective-permute-done | bytes 131104 | tf_op jit(solution)/shard_map/ppermute | solution.py:53
  40.9 8.6 %collective-permute-done.3 = bf16[128,512]{0,1:T(8,128)(2,1)S(1)} collective-permute-done((bf16[128,512]{0,1:T(8,128)(2,1)S(1)}, bf16[128,512]{0,1:T(8,128)(2,1)S(1)}, u32[]{:S(2)}, u32[]{:S(2)}) %collective-permute-start.3) | collective-permute-done | bytes 131104 | tf_op jit(solution)/shard_map/ppermute | solution.py:53
  49.5 8.6 %collective-permute-done.4 = bf16[128,512]{0,1:T(8,128)(2,1)S(1)} collective-permute-done((bf16[128,512]{0,1:T(8,128)(2,1)S(1)}, bf16[128,512]{0,1:T(8,128)(2,1)S(1)}, u32[]{:S(2)}, u32[]{:S(2)}) %collective-permute-start.4) | collective-permute-done | bytes 131104 | tf_op jit(solution)/shard_map/ppermute | solution.py:53
  58.0 8.6 %collective-permute-done.5 = bf16[128,512]{0,1:T(8,128)(2,1)S(1)} collective-permute-done((bf16[128,512]{0,1:T(8,128)(2,1)S(1)}, bf16[128,512]{0,1:T(8,128)(2,1)S(1)}, u32[]{:S(2)}, u32[]{:S(2)}) %collective-permute-start.5) | collective-permute-done | bytes 131104 | tf_op jit(solution)/shard_map/ppermute | solution.py:53
  66.6 9.7 %collective-permute-done.6 = bf16[128,512]{0,1:T(8,128)(2,1)S(1)} collective-permute-done((bf16[128,512]{0,1:T(8,128)(2,1)S(1)}, bf16[128,512]{0,1:T(8,128)(2,1)S(1)}, u32[]{:S(2)}, u32[]{:S(2)}) %collective-permute-start.6) | collective-permute-done | bytes 131104 | tf_op jit(solution)/shard_map/ppermute | solution.py:53
  76.5 8.9 %collective-permute-done.7 = bf16[128,512]{0,1:T(8,128)(2,1)S(1)} collective-permute-done((bf16[128,512]{0,1:T(8,128)(2,1)S(1)}, bf16[128,512]{0,1:T(8,128)(2,1)S(1)}, u32[]{:S(2)}, u32[]{:S(2)}) %collective-permute-start.7) | collective-permute-done | bytes 131104 | tf_op jit(solution)/shard_map/ppermute | solution.py:53
  85.5 8.5 %collective-permute-done.8 = bf16[128,512]{0,1:T(8,128)(2,1)S(1)} collective-permute-done((bf16[128,512]{0,1:T(8,128)(2,1)S(1)}, bf16[128,512]{0,1:T(8,128)(2,1)S(1)}, u32[]{:S(2)}, u32[]{:S(2)}) %collective-permute-start.8) | collective-permute-done | bytes 131104 | tf_op jit(solution)/shard_map/ppermute | solution.py:53
  94.1 8.5 %collective-permute-done.9 = bf16[128,512]{0,1:T(8,128)(2,1)S(1)} collective-permute-done((bf16[128,512]{0,1:T(8,128)(2,1)S(1)}, bf16[128,512]{0,1:T(8,128)(2,1)S(1)}, u32[]{:S(2)}, u32[]{:S(2)}) %collective-permute-start.9) | collective-permute-done | bytes 131104 | tf_op jit(solution)/shard_map/ppermute | solution.py:53
  102.6 8.6 %collective-permute-done.10 = bf16[128,512]{0,1:T(8,128)(2,1)S(1)} collective-permute-done((bf16[128,512]{0,1:T(8,128)(2,1)S(1)}, bf16[128,512]{0,1:T(8,128)(2,1)S(1)}, u32[]{:S(2)}, u32[]{:S(2)}) %collective-permute-start.10) | collective-permute-done | bytes 131104 | tf_op jit(solution)/shard_map/ppermute | solution.py:53
  111.3 8.4 %collective-permute-done.11 = bf16[128,512]{0,1:T(8,128)(2,1)S(1)} collective-permute-done((bf16[128,512]{0,1:T(8,128)(2,1)S(1)}, bf16[128,512]{0,1:T(8,128)(2,1)S(1)}, u32[]{:S(2)}, u32[]{:S(2)}) %collective-permute-start.11) | collective-permute-done | bytes 131104 | tf_op jit(solution)/shard_map/ppermute | solution.py:53
  119.8 8.7 %collective-permute-done.12 = bf16[128,512]{0,1:T(8,128)(2,1)S(1)} collective-permute-done((bf16[128,512]{0,1:T(8,128)(2,1)S(1)}, bf16[128,512]{0,1:T(8,128)(2,1)S(1)}, u32[]{:S(2)}, u32[]{:S(2)}) %collective-permute-start.12) | collective-permute-done | bytes 131104 | tf_op jit(solution)/shard_map/ppermute | solution.py:53
  128.6 8.5 %collective-permute-done.13 = bf16[128,512]{0,1:T(8,128)(2,1)S(1)} collective-permute-done((bf16[128,512]{0,1:T(8,128)(2,1)S(1)}, bf16[128,512]{0,1:T(8,128)(2,1)S(1)}, u32[]{:S(2)}, u32[]{:S(2)}) %collective-permute-start.13) | collective-permute-done | bytes 131104 | tf_op jit(solution)/shard_map/ppermute | solution.py:53
  138.2 7.5 %collective-permute-done.14 = bf16[128,512]{0,1:T(8,128)(2,1)S(1)} collective-permute-done((bf16[128,512]{0,1:T(8,128)(2,1)S(1)}, bf16[128,512]{0,1:T(8,128)(2,1)S(1)}, u32[]{:S(2)}, u32[]{:S(2)}) %collective-permute-start.14) | collective-permute-done | bytes 131104 | tf_op jit(solution)/shard_map/ppermute | solution.py:53
  148.7 2.5 %multiply_reduce_fusion = (f32[4,4,128]{2,1,0:T(4,128)S(1)}, f32[4,4,128,2048]{3,2,1,0:T(8,128)S(1)}) fusion(bf16[4,4,128,64]{2,3,1,0:T(8,128)(2,1)S(1)} %bitcast.38, bf16[2048,4,64,1]{0,2,3,1:T(8,128)(2,1)S(1)} %bitcast.36), kind=kOutput, calls=%fused_computation.1 | convolution fusion | flops 545257472 | bytes 18096128 | tf_op jit(solution)/shard_map/kgqd,nkd->kgqn/dot_general | solution.py:64
  151.2 3.3 %fusion = f32[4,4,128]{2,1,0:T(4,128)S(1)} fusion(f32[4,4,128,2048]{3,2,1,0:T(8,128)S(1)} %get-tuple-element.20, f32[4,4,128]{2,1,0:T(4,128)S(1)} %broadcast_maximum_fusion), kind=kLoop, calls=%fused_computation.2 | loop fusion | flops 12580864 | bytes 16793600 | tf_op jit(solution)/shard_map/reduce_sum | solution.py:68
  154.4 2.5 %copy-done = f32[4,4,128,2048]{3,2,1,0:T(8,128)} copy-done((f32[4,4,128,2048]{3,2,1,0:T(8,128)}, f32[4,4,128,2048]{3,2,1,0:T(8,128)S(1)}, u32[]{:S(2)}) %copy-start) | copy-done | bytes 16777240
  156.9 8.8 %fusion.22 = bf16[128,4,4,64]{0,3,2,1:T(8,128)(2,1)S(1)} fusion(bf16[2048,4,64,1]{0,2,3,1:T(8,128)(2,1)S(1)} %bitcast.39, f32[4,4,128,2048]{3,2,1,0:T(8,128)} %copy-done, f32[4,4,128]{2,1,0:T(4,128)S(1)} %broadcast_maximum_fusion, f32[128,4,4]{0,2,1:T(4,128)S(1)} %bitcast.41), kind=kOutput, calls=%fused_computation.22 | convolution fusion | flops 549715968 | bytes 18104320 | tf_op jit(solution)/shard_map/kgqn,nkd->kgqd/dot_general | solution.py:69
  165.7 3.7 %convolution_convert_fusion = bf16[128,2048]{1,0:T(8,128)(2,1)} fusion(bf16[128,1024]{0,1:T(8,128)(2,1)S(1)} %bitcast.40, bf16[1024,2048]{1,0:T(8,128)(2,1)} %param.11), kind=kOutput, calls=%fused_computation.12 | convolution fusion | flops 537133056 | bytes 4980736 | tf_op jit(solution)/shard_map/dot_general | solution.py:79
  169.5 4.0 %reduce-scatter.2.cloned.1.call-done = bf16[64,2048]{1,0:T(8,128)(2,1)} async-done(((bf16[128,2048]{1,0:T(8,128)(2,1)}), bf16[64,2048]{1,0:T(8,128)(2,1)}) %reduce-scatter.2.cloned.1.call-update) | async-done | bytes 262160 | tf_op jit(solution)/shard_map/reduce_scatter | solution.py:78
  (76 shorter events, 4.5 us)
Async XLA Ops:
  6.5 166.9 %reduce-scatter.2.cloned.1.call-start = ((), (), s32[]{:S(2)}) async-start(), calls=%async_computation.1 | async-start | bytes 786432 | tf_op jit(solution)/shard_map/reduce_scatter | solution.py:78
  9.0 67.4 %copy-start.1 = (f32[64]{0:T(128)S(1)}, f32[64]{0:T(128)}, u32[]{:S(2)}) copy-start(f32[64]{0:T(128)} %param.12) | copy-start | bytes 772
  13.1 125.0 %copy-start.2 = (f32[64]{0:T(128)S(1)}, f32[64]{0:T(128)}, u32[]{:S(2)}) copy-start(f32[64]{0:T(128)} %param.13) | copy-start | bytes 772
  13.1 10.7 %collective-permute-start = (bf16[128,512]{0,1:T(8,128)(2,1)S(1)}, bf16[128,512]{0,1:T(8,128)(2,1)S(1)}, u32[]{:S(2)}, u32[]{:S(2)}) collective-permute-start(bf16[128,512]{0,1:T(8,128)(2,1)S(1)} %concatenate.31), channel_id=1, source_target_pairs={{0,2},{2,4},{4,6},{6,8},{8,10},{10,12},{12,14},{14,16},{16,18},{18... | collective-permute-start | bytes 393224 | tf_op jit(solution)/shard_map/ppermute | solution.py:53
  23.8 8.6 %collective-permute-start.1 = (bf16[128,512]{0,1:T(8,128)(2,1)S(1)}, bf16[128,512]{0,1:T(8,128)(2,1)S(1)}, u32[]{:S(2)}, u32[]{:S(2)}) collective-permute-start(bf16[128,512]{0,1:T(8,128)(2,1)S(1)} %collective-permute-done), channel_id=1, source_target_pairs={{0,2},{2,4},{4,6},{6,8},{8,10},{10,12},{12,14},{14,16},{16,18},{18... | collective-permute-start | bytes 393224 | tf_op jit(solution)/shard_map/ppermute | solution.py:53
  32.4 8.6 %collective-permute-start.2 = (bf16[128,512]{0,1:T(8,128)(2,1)S(1)}, bf16[128,512]{0,1:T(8,128)(2,1)S(1)}, u32[]{:S(2)}, u32[]{:S(2)}) collective-permute-start(bf16[128,512]{0,1:T(8,128)(2,1)S(1)} %collective-permute-done.1), channel_id=1, source_target_pairs={{0,2},{2,4},{4,6},{6,8},{8,10},{10,12},{12,14},{14,16},{16,18},{18... | collective-permute-start | bytes 393224 | tf_op jit(solution)/shard_map/ppermute | solution.py:53
  40.9 8.6 %collective-permute-start.3 = (bf16[128,512]{0,1:T(8,128)(2,1)S(1)}, bf16[128,512]{0,1:T(8,128)(2,1)S(1)}, u32[]{:S(2)}, u32[]{:S(2)}) collective-permute-start(bf16[128,512]{0,1:T(8,128)(2,1)S(1)} %collective-permute-done.2), channel_id=1, source_target_pairs={{0,2},{2,4},{4,6},{6,8},{8,10},{10,12},{12,14},{14,16},{16,18},{18... | collective-permute-start | bytes 393224 | tf_op jit(solution)/shard_map/ppermute | solution.py:53
  49.5 8.6 %collective-permute-start.4 = (bf16[128,512]{0,1:T(8,128)(2,1)S(1)}, bf16[128,512]{0,1:T(8,128)(2,1)S(1)}, u32[]{:S(2)}, u32[]{:S(2)}) collective-permute-start(bf16[128,512]{0,1:T(8,128)(2,1)S(1)} %collective-permute-done.3), channel_id=1, source_target_pairs={{0,2},{2,4},{4,6},{6,8},{8,10},{10,12},{12,14},{14,16},{16,18},{18... | collective-permute-start | bytes 393224 | tf_op jit(solution)/shard_map/ppermute | solution.py:53
  58.0 8.6 %collective-permute-start.5 = (bf16[128,512]{0,1:T(8,128)(2,1)S(1)}, bf16[128,512]{0,1:T(8,128)(2,1)S(1)}, u32[]{:S(2)}, u32[]{:S(2)}) collective-permute-start(bf16[128,512]{0,1:T(8,128)(2,1)S(1)} %collective-permute-done.4), channel_id=1, source_target_pairs={{0,2},{2,4},{4,6},{6,8},{8,10},{10,12},{12,14},{14,16},{16,18},{18... | collective-permute-start | bytes 393224 | tf_op jit(solution)/shard_map/ppermute | solution.py:53
  66.6 9.7 %collective-permute-start.6 = (bf16[128,512]{0,1:T(8,128)(2,1)S(1)}, bf16[128,512]{0,1:T(8,128)(2,1)S(1)}, u32[]{:S(2)}, u32[]{:S(2)}) collective-permute-start(bf16[128,512]{0,1:T(8,128)(2,1)S(1)} %collective-permute-done.5), channel_id=1, source_target_pairs={{0,2},{2,4},{4,6},{6,8},{8,10},{10,12},{12,14},{14,16},{16,18},{18... | collective-permute-start | bytes 393224 | tf_op jit(solution)/shard_map/ppermute | solution.py:53
  76.3 9.1 %collective-permute-start.7 = (bf16[128,512]{0,1:T(8,128)(2,1)S(1)}, bf16[128,512]{0,1:T(8,128)(2,1)S(1)}, u32[]{:S(2)}, u32[]{:S(2)}) collective-permute-start(bf16[128,512]{0,1:T(8,128)(2,1)S(1)} %collective-permute-done.6), channel_id=1, source_target_pairs={{0,2},{2,4},{4,6},{6,8},{8,10},{10,12},{12,14},{14,16},{16,18},{18... | collective-permute-start | bytes 393224 | tf_op jit(solution)/shard_map/ppermute | solution.py:53
  85.4 8.6 %collective-permute-start.8 = (bf16[128,512]{0,1:T(8,128)(2,1)S(1)}, bf16[128,512]{0,1:T(8,128)(2,1)S(1)}, u32[]{:S(2)}, u32[]{:S(2)}) collective-permute-start(bf16[128,512]{0,1:T(8,128)(2,1)S(1)} %collective-permute-done.7), channel_id=1, source_target_pairs={{0,2},{2,4},{4,6},{6,8},{8,10},{10,12},{12,14},{14,16},{16,18},{18... | collective-permute-start | bytes 393224 | tf_op jit(solution)/shard_map/ppermute | solution.py:53
  94.0 8.6 %collective-permute-start.9 = (bf16[128,512]{0,1:T(8,128)(2,1)S(1)}, bf16[128,512]{0,1:T(8,128)(2,1)S(1)}, u32[]{:S(2)}, u32[]{:S(2)}) collective-permute-start(bf16[128,512]{0,1:T(8,128)(2,1)S(1)} %collective-permute-done.8), channel_id=1, source_target_pairs={{0,2},{2,4},{4,6},{6,8},{8,10},{10,12},{12,14},{14,16},{16,18},{18... | collective-permute-start | bytes 393224 | tf_op jit(solution)/shard_map/ppermute | solution.py:53
  102.6 8.6 %collective-permute-start.10 = (bf16[128,512]{0,1:T(8,128)(2,1)S(1)}, bf16[128,512]{0,1:T(8,128)(2,1)S(1)}, u32[]{:S(2)}, u32[]{:S(2)}) collective-permute-start(bf16[128,512]{0,1:T(8,128)(2,1)S(1)} %collective-permute-done.9), channel_id=1, source_target_pairs={{0,2},{2,4},{4,6},{6,8},{8,10},{10,12},{12,14},{14,16},{16,18},{18... | collective-permute-start | bytes 393224 | tf_op jit(solution)/shard_map/ppermute | solution.py:53
  111.1 8.6 %collective-permute-start.11 = (bf16[128,512]{0,1:T(8,128)(2,1)S(1)}, bf16[128,512]{0,1:T(8,128)(2,1)S(1)}, u32[]{:S(2)}, u32[]{:S(2)}) collective-permute-start(bf16[128,512]{0,1:T(8,128)(2,1)S(1)} %collective-permute-done.10), channel_id=1, source_target_pairs={{0,2},{2,4},{4,6},{6,8},{8,10},{10,12},{12,14},{14,16},{16,18},{18... | collective-permute-start | bytes 393224 | tf_op jit(solution)/shard_map/ppermute | solution.py:53
  119.7 8.9 %collective-permute-start.12 = (bf16[128,512]{0,1:T(8,128)(2,1)S(1)}, bf16[128,512]{0,1:T(8,128)(2,1)S(1)}, u32[]{:S(2)}, u32[]{:S(2)}) collective-permute-start(bf16[128,512]{0,1:T(8,128)(2,1)S(1)} %collective-permute-done.11), channel_id=1, source_target_pairs={{0,2},{2,4},{4,6},{6,8},{8,10},{10,12},{12,14},{14,16},{16,18},{18... | collective-permute-start | bytes 393224 | tf_op jit(solution)/shard_map/ppermute | solution.py:53
  128.5 8.6 %collective-permute-start.13 = (bf16[128,512]{0,1:T(8,128)(2,1)S(1)}, bf16[128,512]{0,1:T(8,128)(2,1)S(1)}, u32[]{:S(2)}, u32[]{:S(2)}) collective-permute-start(bf16[128,512]{0,1:T(8,128)(2,1)S(1)} %collective-permute-done.12), channel_id=1, source_target_pairs={{0,2},{2,4},{4,6},{6,8},{8,10},{10,12},{12,14},{14,16},{16,18},{18... | collective-permute-start | bytes 393224 | tf_op jit(solution)/shard_map/ppermute | solution.py:53
  137.1 8.6 %collective-permute-start.14 = (bf16[128,512]{0,1:T(8,128)(2,1)S(1)}, bf16[128,512]{0,1:T(8,128)(2,1)S(1)}, u32[]{:S(2)}, u32[]{:S(2)}) collective-permute-start(bf16[128,512]{0,1:T(8,128)(2,1)S(1)} %collective-permute-done.13), channel_id=1, source_target_pairs={{0,2},{2,4},{4,6},{6,8},{8,10},{10,12},{12,14},{14,16},{16,18},{18... | collective-permute-start | bytes 393224 | tf_op jit(solution)/shard_map/ppermute | solution.py:53
  151.1 5.7 %copy-start = (f32[4,4,128,2048]{3,2,1,0:T(8,128)}, f32[4,4,128,2048]{3,2,1,0:T(8,128)S(1)}, u32[]{:S(2)}) copy-start(f32[4,4,128,2048]{3,2,1,0:T(8,128)S(1)} %get-tuple-element.20) | copy-start | bytes 50331652
Sparse Core Ops, SparseCore 0:
  169.6 3.7 reduce-scatter.1
